TPU v7x, 32 devices: a whole 2x2x4 slice. The times are simulated.
32 devices in a mesh: fs: 8 (over z, y), tp: 4 (over x, core).
Axes of the slice: x: 2, y: 2, z: 4, core: 2. Of those that a mesh axis runs over, the one named last changes fastest.
Arguments:
- cotangent: bfloat16 [5120, 1024], P('fs', 'tp'), may hold values from -6 to 6
- inputs: bfloat16 [5120, 1024], P('fs', 'tp'), may hold values from -6 to 6
- pre_act: bfloat16 [5120, 2112], P('fs'), may hold values from -6 to 6
- w_up: bfloat16 [2112, 1024], P('fs', 'tp'), may hold values from -0.1875 to 0.1875
- w_down: bfloat16 [2112, 1024], P('fs', 'tp'), may hold values from -0.125 to 0.125
Outputs:
- grad_input: bfloat16 [5120, 1024], P('fs', 'tp')
- grad_up: float32 [2112, 1024], P('fs', 'tp')
All inputs are finite; a program needn't handle non-finite values.
Results may differ from a plain program's by a relative error of at most 0.0049.
Values may be sent and summed in bfloat16 or wider, within the bound.
A program may use at most 64 MiB of HBM per device.

v0:
```python
import functools

import jax
import jax.numpy as jnp
from jax import lax
from jax.experimental import pallas as pl
from jax.experimental.pallas import tpu as pltpu
from jax.sharding import PartitionSpec as P

MESH = pl.DeviceIdType.MESH


def times_rows(left, piece):
    return lax.dot_general(
        left, piece, (((1,), (1,)), ((), ())), preferred_element_type=jnp.float32
    )


def toggled(index, mask, bits):
    for bit in range(bits):
        unit = 2**bit
        index = index + unit * ((mask // unit) % 2) * (1 - 2 * ((index // unit) % 2))
    return index


def kernel(
    n, token_total,
    cot_ref, in_ref, pre_ref, up_ref, down_ref,
    gi_ref, gu_ref,
    cot_buf, cot_turned, down_buf, up_buf, pre_buf, held, y_out, y_in, z_out, z_in,
    local_sem, cot_send, cot_recv, dz_send, dy_send, dx_send, dc_send, dr_send, down_recv,
    uz_send, uy_send, up_recv, ys_send, ys_recv, zs_send, zs_recv,
):
    bits = n.bit_length() - 1
    half = n // 2
    f = lax.axis_index("fs")
    t = lax.axis_index("tp")
    width = cot_ref.shape[1]
    t_core = toggled(t, 1, 2)
    t_x = toggled(t, 2, 2)
    t_xcore = toggled(t, 3, 2)
    f_y = toggled(f, 1, 1)

    def split(i):
        pair = i // 2
        last = pair // (half - 1)
        return (pair + 1) % half, i % 2 + last * (1 - 2 * (i % 2))

    def seq(i):
        far, across = split(i)
        return toggled(f, 2 * far + across, bits)

    def cols(tp):
        return pl.ds(pl.multiple_of(tp * width, width), width)

    def down_slot(src_f, src_t):
        return down_buf.at[src_f, :, cols(src_t)]

    def remote(src, dst, send, recv, fs, tp):
        return pltpu.make_async_remote_copy(
            src_ref=src, dst_ref=dst, send_sem=send, recv_sem=recv,
            device_id=(fs, tp), device_id_type=MESH,
        )

    def cot_copy(src, src_t, slot, tp):
        return remote(src, cot_buf.at[:, cols(src_t)], cot_send.at[slot], cot_recv.at[src_t], f, tp)

    def down_copy(src, src_f, src_t, send, fs, tp):
        return remote(src, down_slot(src_f, src_t), send, down_recv.at[src_f, src_t], fs, tp)

    def up_copy(src, src_f, send, fs):
        return remote(src, up_buf.at[src_f], send, up_recv.at[src_f], fs, t)

    def y_copy(pair):
        return remote(y_out.at[pair], y_in.at[pair], ys_send.at[pair], ys_recv.at[pair], f_y, t)

    def z_copy(pair):
        owner = toggled(f, 2 * (pair + 1), bits)
        return remote(z_out.at[pair], z_in.at[pair], zs_send.at[pair], zs_recv.at[pair], owner, t)

    local = [
        pltpu.make_async_copy(cot_ref, cot_buf.at[:, cols(t)], local_sem.at[0]),
        pltpu.make_async_copy(down_ref, down_slot(f, t), local_sem.at[1]),
        pltpu.make_async_copy(up_ref, up_buf.at[f], local_sem.at[2]),
        pltpu.make_async_copy(pre_ref, pre_buf, local_sem.at[3]),
    ]
    for copy in local:
        copy.start()

    barrier = pltpu.get_barrier_semaphore()
    far_peers = [toggled(f, 2 * k, bits) for k in range(1, half)]
    peers = [(peer, t) for peer in far_peers] + [(f_y, t), (f, t_core), (f, t_x)]
    for peer in peers:
        pl.semaphore_signal(barrier, inc=1, device_id=peer, device_id_type=MESH)
    pl.semaphore_wait(barrier, len(peers))

    sent = []

    def go(copy):
        copy.start()
        sent.append(copy)

    go(cot_copy(cot_ref, t, 1, t_x))
    for k in range(1, half):
        go(down_copy(down_ref, f, t, dz_send.at[k], far_peers[k - 1], t))
    go(down_copy(down_ref, f, t, dy_send.at[0], f_y, t))
    go(cot_copy(cot_ref, t, 0, t_core))

    def arrived_down(src_f, src_t):
        down_copy(down_slot(src_f, src_t), src_f, src_t, dz_send.at[0], f, t_core).wait_recv()

    def arrived_up(src_f):
        up_copy(up_buf.at[src_f], src_f, uz_send.at[0], f_y).wait_recv()

    def arrived_cot(src_t):
        cot_copy(cot_buf.at[:, cols(src_t)], src_t, 0, t_core).wait_recv()

    def take_own(i):
        far, across = split(i)
        src = seq(i)

        @pl.when(far + across > 0)
        def _():
            arrived_down(src, t)

        block = down_slot(src, t)
        down_copy(block, src, t, dx_send.at[i], f, t_x).start()
        down_copy(block, src, t, dc_send.at[i], f, t_core).start()

        @pl.when((far > 0) & (across == 0))
        def _():
            down_copy(block, src, t, dy_send.at[far], f_y, t).start()

    local[1].wait()
    take_own(0)
    arrived_cot(t_x)
    go(cot_copy(cot_buf.at[:, cols(t_x)], t_x, 2, t_core))
    take_own(1)
    for k in range(1, half):
        go(up_copy(up_ref, f, uz_send.at[k], far_peers[k - 1]))
    go(up_copy(up_ref, f, uy_send.at[0], f_y))
    local[0].wait()
    arrived_cot(t_core)
    arrived_cot(t_xcore)
    cot_turned[...] = cot_buf[...].T
    local[2].wait()
    local[3].wait()

    def step(i, carry):
        @pl.when((i < n - 1) & (i > 0))
        def _():
            take_own(i + 1)

        @pl.when(i < n)
        def _():
            src = seq(i)
            arrived_down(src, t_x)
            down_copy(down_slot(src, t_x), src, t_x, dr_send.at[i], f, t_core).start()

        @pl.when((i >= 3) & (i < half + 2))
        def _():
            k = i - 2
            src = toggled(f, 2 * k, bits)
            arrived_up(src)
            up_copy(up_buf.at[src], src, uy_send.at[k], f_y).start()

        @pl.when(i > 0)
        def _():
            j = i - 1
            src = seq(j)
            pair = j // 2
            arrived_down(src, t_core)
            arrived_down(src, t_xcore)
            hidden = jnp.dot(down_buf[src], cot_turned[...], preferred_element_type=jnp.float32)
            grad_pre = (
                2.0 * hidden * jnp.maximum(pre_buf[src].astype(jnp.float32), 0.0)
            ).astype(jnp.bfloat16)
            pre_buf[src] = grad_pre
            part = jnp.dot(grad_pre, in_ref[...], preferred_element_type=jnp.float32)
            _, across = split(j)

            @pl.when(across == 0)
            def _():
                held[pair] = part

            @pl.when(across == 1)
            def _():
                y_out[pair] = part.astype(jnp.bfloat16)
                y_copy(pair).start()

        @pl.when((i >= 3) & (i % 2 == 1))
        def _():
            pair = (i - 3) // 2
            y_copy(pair).wait_recv()
            z_out[pair] = (held[pair] + y_in[pair].astype(jnp.float32)).astype(jnp.bfloat16)
            z_copy(pair).start()

        return carry

    lax.fori_loop(0, n + 1, step, 0)

    for k in range(half):
        arrived_up(toggled(f, 2 * k + 1, bits))
    gi = jnp.zeros(gi_ref.shape, jnp.float32)
    for block in range(n):
        gi = gi + lax.dot_general(
            pre_buf[block], up_buf[block], (((0,), (0,)), ((), ())),
            preferred_element_type=jnp.float32,
        )
    gi_ref[...] = gi.astype(gi_ref.dtype)

    total = held[half - 1]
    for pair in range(half - 1):
        z_copy(pair).wait_recv()
        total = total + z_in[pair].astype(jnp.float32)
    y_copy(half - 1).wait_recv()
    total = total + y_in[half - 1].astype(jnp.float32)
    gu_ref[...] = total / jnp.sqrt(jnp.float32(token_total))

    for copy in sent:
        copy.wait_send()
    for i in range(n):
        src = seq(i)
        far, across = split(i)
        block = down_slot(src, t)
        down_copy(block, src, t, dx_send.at[i], f, t_x).wait_send()
        down_copy(block, src, t, dc_send.at[i], f, t_core).wait_send()
        down_copy(down_slot(src, t_x), src, t_x, dr_send.at[i], f, t_core).wait_send()
        if far > 0 and across == 0:
            down_copy(block, src, t, dy_send.at[far], f_y, t).wait_send()
            up_copy(up_buf.at[src], src, uy_send.at[far], f_y).wait_send()
    for pair in range(half):
        y_copy(pair).wait_send()
        if pair < half - 1:
            z_copy(pair).wait_send()


def settle(gi_ref, gu_ref, gi_out, gu_out):
    gi_out[...] = gi_ref[...]
    gu_out[...] = gu_ref[...]


def fused(n, tp, cotangent, inputs, pre_act, w_up, w_down):
    tokens, width = cotangent.shape
    rows = w_down.shape[0]
    dma = pltpu.SemaphoreType.DMA
    half = n // 2
    vmem = pl.BlockSpec(memory_space=pltpu.VMEM)
    shapes = (
        jax.ShapeDtypeStruct((tokens, width), jnp.bfloat16),
        jax.ShapeDtypeStruct((rows, width), jnp.float32),
    )
    results = pl.pallas_call(
        functools.partial(kernel, n, tokens * n),
        out_shape=shapes,
        in_specs=[vmem, vmem, pl.BlockSpec(memory_space=pl.ANY), vmem, vmem],
        out_specs=(vmem, vmem),
        scratch_shapes=[
            pltpu.VMEM((tokens, tp * width), jnp.bfloat16),
            pltpu.VMEM((tp * width, tokens), jnp.bfloat16),
            pltpu.VMEM((n, rows, tp * width), jnp.bfloat16),
            pltpu.VMEM((n, rows, width), jnp.bfloat16),
            pltpu.VMEM((n, rows, tokens), jnp.bfloat16),
            pltpu.VMEM((half, rows, width), jnp.float32),
            pltpu.VMEM((half, rows, width), jnp.bfloat16),
            pltpu.VMEM((half, rows, width), jnp.bfloat16),
            pltpu.VMEM((half - 1, rows, width), jnp.bfloat16),
            pltpu.VMEM((half - 1, rows, width), jnp.bfloat16),
            dma((4,)),
            dma((3,)), dma((tp,)),
            dma((half,)), dma((half,)), dma((n,)), dma((n,)), dma((n,)), dma((n, tp)),
            dma((half,)), dma((half,)), dma((n,)),
            dma((half,)), dma((half,)), dma((half - 1,)), dma((half - 1,)),
        ],
        compiler_params=pltpu.CompilerParams(
            collective_id=0, has_side_effects=True, vmem_limit_bytes=60 * 2**20
        ),
    )(cotangent, inputs, pre_act.T.reshape(n, rows, tokens), w_up, w_down)
    return pl.pallas_call(
        settle, out_shape=shapes, in_specs=[vmem, vmem], out_specs=(vmem, vmem)
    )(*results)


def gathered(cotangent, inputs, pre_act, w_up, w_down):
    token_total = cotangent.shape[0] * lax.axis_size("fs")
    full_cotangent = lax.all_gather(cotangent, "tp", axis=1, tiled=True)
    down_whole = lax.all_gather(w_down, "tp", axis=1, tiled=True)
    grad_hidden = times_rows(full_cotangent, lax.all_gather(down_whole, "fs", axis=0, tiled=True))
    grad_pre = (2.0 * grad_hidden * jnp.maximum(pre_act.astype(jnp.float32), 0.0)).astype(
        jnp.bfloat16
    )
    grad_input = jnp.dot(
        grad_pre, lax.all_gather(w_up, "fs", axis=0, tiled=True), preferred_element_type=jnp.float32
    )
    grad_share = lax.psum_scatter(
        lax.dot_general(
            grad_pre, inputs, (((0,), (0,)), ((), ())), preferred_element_type=jnp.float32
        ),
        "fs",
        scatter_dimension=0,
        tiled=True,
    )
    grad_up = grad_share / jnp.sqrt(jnp.float32(token_total))
    return (grad_input.astype(jnp.bfloat16), grad_up)


def solution(mesh):
    n, tp = mesh.shape["fs"], mesh.shape["tp"]

    def local(cotangent, inputs, pre_act, w_up, w_down):
        rows, width = w_down.shape
        fits = tp == 4 and 4 <= n <= 16 and n & (n - 1) == 0 and rows % 8 == 0 and width % 128 == 0
        if fits:
            return fused(n, tp, cotangent, inputs, pre_act, w_up, w_down)
        return gathered(cotangent, inputs, pre_act, w_up, w_down)

    return jax.shard_map(
        local,
        mesh=mesh,
        in_specs=(P("fs", "tp"), P("fs", "tp"), P("fs", None), P("fs", "tp"), P("fs", "tp")),
        out_specs=(P("fs", "tp"), P("fs", "tp")),
        check_vma=False,
    )
```

profile of v0, /device:TPU:0, one launch (start us, length us, event | category | flops | bytes accessed | tf_op | source)
XLA Modules:
  0.0 56.7 jit_solution(11735716505512569928)
XLA Ops:
  0.6 54.2 %shard_map.68 = (bf16[640,256]{1,0:T(8,128)(2,1)}, f32[264,256]{1,0:T(8,128)}) custom-call(bf16[640,256]{1,0:T(8,128)(2,1)} %cot_ref.1, bf16[640,256]{1,0:T(8,128)(2,1)} %in_ref.1, bf16[8,264,640]{2,1,0:T(8,128)(2,1)} %bitcast.3, bf16[264,256]{1,0:T(8,128)(2,1)} %up_ref.1, bf16[264,256]{1,0:T(8,128)(2,1)} %down_ref.1), custom_call_target="tpu_custom_call" | custom-call | tf_op jit(solution)/shard_map/pallas_call | solution.py:253
  54.9 1.9 %shard_map.69 = (bf16[640,256]{1,0:T(8,128)(2,1)}, f32[264,256]{1,0:T(8,128)}) custom-call(bf16[640,256]{1,0:T(8,128)(2,1)} %get-tuple-element.4.gi_ref, f32[264,256]{1,0:T(8,128)} %get-tuple-element.5.gu_ref), custom_call_target="tpu_custom_call" | custom-call | tf_op jit(solution)/shard_map/pallas_call | solution.py:279
where the time goes:
time: 56.9 us; the launch traced here: 56.7 us
  Pallas kernels  56.1 us (99%)
  between operations  0.64 us (1%)
    pallas_call x1, Pallas kernels, fused(): pl.pallas_call(functools.partial(kernel, n, tokens * n), out_shape=shapes...  54.2 us
    pallas_call x1, Pallas kernels, fused(): pl.pallas_call(settle, out_shape=shapes, in_specs=[vmem, vmem], out_specs...  1.89 us

commit v1 on v0

v1 whole, which is shorter than its diff:
```python
import functools

import jax
import jax.numpy as jnp
from jax import lax
from jax.experimental import pallas as pl
from jax.experimental.pallas import tpu as pltpu
from jax.sharding import PartitionSpec as P

MESH = pl.DeviceIdType.MESH
MIDDLE = 8
LAG = 3


def times_rows(left, piece):
    return lax.dot_general(
        left, piece, (((1,), (1,)), ((), ())), preferred_element_type=jnp.float32
    )


def kernel(
    n, token_total,
    cot_hbm, in_hbm, pre_hbm, up_hbm, down_hbm,
    gi_ref, gu_ref,
    cot_buf, cot_turned, in_buf, down_buf, swap_buf, up_buf, pre_buf, grad, held,
    out_buf, in_sum, y_in,
    local_sem, cot_send, cot_recv, swap_send, dz_send, dy_send, dc_send, down_recv,
    uz_send, uy_send, up_recv, gx_send, gx_recv, gc_send, gc_recv,
    rs_send, rs_recv, y_recv,
):
    deep = n // 2
    f = lax.axis_index("fs")
    t = lax.axis_index("tp")
    z, y = f // 2, f % 2
    x, c = t // 2, t % 2
    width = in_buf.shape[1]
    rows = up_buf.shape[1]
    main = (rows - MIDDLE) // 2
    half = main // 2
    own_rows = main + MIDDLE
    t_core = t + 1 - 2 * c
    t_x = t + 2 - 4 * x
    t_xcore = t_core + 2 - 4 * x
    f_y = f + 1 - 2 * y
    is_end = (z == 0) | (z == deep - 1)

    def cols(tp):
        return pl.ds(pl.multiple_of(tp * width, width), width)

    def seq(i):
        p, q = i // 2, i % 2
        flip = z // 2
        near = z + flip * (deep - 1 - 2 * z)
        v = deep - 1 - p + near * (p // 2) * (2 * p - 5)
        return 2 * (v + flip * (deep - 1 - 2 * v)) + (1 - q) * (1 - y) + q * y

    def remote(src, dst, send, recv, fs, tp):
        return pltpu.make_async_remote_copy(
            src_ref=src, dst_ref=dst, send_sem=send, recv_sem=recv,
            device_id=(fs, tp), device_id_type=MESH,
        )

    lower = pl.ds(pl.multiple_of((main + MIDDLE) * x, 8), main)
    other = pl.ds(pl.multiple_of((main + MIDDLE) * (1 - x), 8), main)
    middle = pl.ds(main, MIDDLE)
    first, second, last = pl.ds(0, main), pl.ds(main, main), pl.ds(2 * main, MIDDLE)

    plan = [
        (down_hbm.at[other], swap_buf.at[first]),
        (down_hbm.at[middle], swap_buf.at[middle]),
        (down_hbm.at[lower], down_buf.at[f, first, cols(t)]),
        (down_hbm.at[middle], down_buf.at[f, middle, cols(t)]),
        (cot_hbm, cot_buf.at[:, cols(t)]),
        (up_hbm.at[lower], up_buf.at[f, first]),
        (up_hbm.at[other], up_buf.at[f, second]),
        (up_hbm.at[middle], up_buf.at[f, last]),
        (in_hbm, in_buf),
        (pre_hbm.at[:, lower], pre_buf.at[:, first]),
        (pre_hbm.at[:, middle], pre_buf.at[:, middle]),
    ]
    local = [
        pltpu.make_async_copy(src, dst, local_sem.at[k]) for k, (src, dst) in enumerate(plan)
    ]
    for copy in local:
        copy.start()

    def swap_copy():
        return remote(
            swap_buf, down_buf.at[f, :, cols(t)], swap_send.at[0], down_recv.at[f, t], f, t_x
        )

    def cot_copy(src_t, slot, tp):
        block = cot_buf.at[:, cols(src_t)]
        return remote(block, block, cot_send.at[slot], cot_recv.at[src_t], f, tp)

    def piece(k):
        return t if k == 0 else t_x

    def down_copy(src_f, k, send, fs, tp):
        block = down_buf.at[src_f, :, cols(piece(k))]
        return remote(block, block, send, down_recv.at[src_f, piece(k)], fs, tp)

    def down_z(src_f, k, step):
        return down_copy(src_f, k, dz_send.at[(1 + step) // 2, src_f // 2, k], f + 2 * step, t)

    def down_y(src_f, k):
        return down_copy(src_f, k, dy_send.at[src_f // 2, k], f_y, t)

    def down_c(src_f, k):
        return down_copy(src_f, k, dc_send.at[src_f, k], f, t_core)

    def up_copy(src_f, send, fs):
        return remote(up_buf.at[src_f], up_buf.at[src_f], send, up_recv.at[src_f], fs, t)

    def up_z(src_f, step):
        return up_copy(src_f, uz_send.at[(1 + step) // 2, src_f // 2], f + 2 * step)

    def up_y(src_f):
        return up_copy(src_f, uy_send.at[src_f // 2], f_y)

    def grad_x(src_f):
        src = grad.at[src_f, pl.ds(pl.multiple_of(half * c, half), half)]
        dst = grad.at[src_f, pl.ds(pl.multiple_of(main + half * c, half), half)]
        return remote(src, dst, gx_send.at[src_f], gx_recv.at[src_f], f, t_x)

    def grad_c(src_f):
        block = grad.at[src_f, pl.ds(pl.multiple_of(main + half * c, half), half)]
        return remote(block, block, gc_send.at[src_f], gc_recv.at[src_f], f, t_core)

    parts = (pl.ds(0, main), pl.ds(main, own_rows))

    def sum_copy(src_f, part, step):
        return remote(
            out_buf.at[src_f, parts[part]], in_sum.at[(1 - step) // 2, src_f, parts[part]],
            rs_send.at[src_f, part], rs_recv.at[(1 - step) // 2, src_f, part], f + 2 * step, t,
        )

    def y_copy(part):
        return remote(
            out_buf.at[f_y, parts[part]], y_in.at[parts[part]],
            rs_send.at[f_y, part], y_recv.at[part], f_y, t,
        )

    def inside(zz):
        return (zz >= 0) & (zz < deep)

    barrier = pltpu.get_barrier_semaphore()
    for peer in ((f_y, t), (f, t_core), (f, t_x)):
        pl.semaphore_signal(barrier, inc=1, device_id=peer, device_id_type=MESH)
    for step in (-1, 1):
        @pl.when(inside(z + step))
        def _():
            pl.semaphore_signal(barrier, inc=1, device_id=(f + 2 * step, t), device_id_type=MESH)
    for k in range(5):
        local[k].wait()
    pl.semaphore_wait(barrier, 5 - is_end.astype(jnp.int32))

    def forward_down(src_f, k, steps, act):
        for step in steps:
            @pl.when(inside(z + step))
            def _():
                act(down_z(src_f, k, step))
        act(down_y(src_f, k))
        act(down_c(src_f, k))

    def start(copy):
        copy.start()

    def finish(copy):
        copy.wait_send()

    def arrived_down(src_f, tp):
        block = down_buf.at[src_f, :, cols(tp)]
        remote(block, block, swap_send.at[0], down_recv.at[src_f, tp], f, t_core).wait_recv()

    def arrived_cot(src_t):
        cot_copy(src_t, 0, t_core).wait_recv()

    def line(d, k):
        for sign in (-1, 1):
            @pl.when(inside(z + sign * d))
            def _():
                src = f + 2 * sign * d
                arrived_down(src, piece(k))
                forward_down(src, k, (-sign,), start)

    def beside(d, k):
        for sign in (-1, 1) if d else (1,):
            @pl.when(inside(z + sign * d))
            def _():
                src = f_y + 2 * sign * d
                arrived_down(src, piece(k))
                down_c(src, k).start()

    def turn(tp):
        cot_turned[cols(tp)] = cot_buf[:, cols(tp)].T

    swap_copy().start()
    forward_down(f, 0, (-1, 1), start)
    cot_copy(t, 1, t_x).start()
    cot_copy(t, 0, t_core).start()
    turn(t)
    arrived_down(f, t_x)
    forward_down(f, 1, (-1, 1), start)
    line(1, 0)
    beside(0, 0)
    for k in range(5, len(local)):
        local[k].wait()
    arrived_cot(t_core)
    turn(t_core)
    line(1, 1)
    for step in (-1, 1):
        @pl.when(inside(z + step) & (z // 2 == (1 - step) // 2))
        def _():
            up_z(f, step).start()
    beside(0, 1)
    line(2, 0)
    beside(1, 0)
    line(2, 1)
    beside(1, 1)
    arrived_cot(t_x)
    cot_copy(t_x, 2, t_core).start()
    turn(t_x)
    line(3, 0)
    beside(2, 0)
    line(3, 1)
    for step in (-1, 1):
        @pl.when(inside(z + step) & (z // 2 != (1 - step) // 2))
        def _():
            up_z(f, step).start()
    up_y(f).start()
    beside(2, 1)
    beside(3, 0)
    beside(3, 1)
    arrived_cot(t_xcore)
    turn(t_xcore)

    def relay(src, part):
        area = parts[part]
        zd = src // 2

        @pl.when((zd >= z) & (z > 0))
        def _():
            sum_copy(src, part, 1).wait_recv()
            held[src, area] = held[src, area] + in_sum[0, src, area].astype(jnp.float32)

        @pl.when((zd <= z) & (z < deep - 1))
        def _():
            sum_copy(src, part, -1).wait_recv()
            held[src, area] = held[src, area] + in_sum[1, src, area].astype(jnp.float32)

        @pl.when(src != f)
        def _():
            out_buf[src, area] = held[src, area].astype(jnp.bfloat16)

        @pl.when(zd > z)
        def _():
            sum_copy(src, part, 1).start()

        @pl.when(zd < z)
        def _():
            sum_copy(src, part, -1).start()

        @pl.when(src == f_y)
        def _():
            y_copy(part).start()

    def head(src):
        return is_end & (src // 2 != z)

    def produce(i, carry):
        src = seq(i)
        arrived_down(src, t_core)
        arrived_down(src, t_xcore)
        hidden = jnp.dot(down_buf[src], cot_turned[...], preferred_element_type=jnp.float32)
        grad_pre = (
            2.0 * hidden * jnp.maximum(pre_buf[src].astype(jnp.float32), 0.0)
        ).astype(jnp.bfloat16)
        grad[src, first] = grad_pre[:main]
        grad[src, last] = grad_pre[main:]
        grad_x(src).start()
        held[src, first] = jnp.dot(
            grad_pre[:main], in_buf[...], preferred_element_type=jnp.float32
        )

        @pl.when(head(src))
        def _():
            relay(src, 0)

        return carry

    lax.fori_loop(0, n, produce, 0)

    def step(i, carry):
        @pl.when(i < n)
        def _():
            src = seq(i)
            grad_x(src).wait_recv()
            grad_c(src).start()

        for d in range(1, deep):
            for sign in (-1, 1):
                @pl.when((i == 2 * (d - 1)) & inside(z + sign * d))
                def _():
                    src = f + 2 * sign * d
                    up_y(src).wait_recv()
                    up_y(src).start()

                    @pl.when(inside(z - sign))
                    def _():
                        up_z(src, -sign).start()

        @pl.when((i > 0) & (i <= n))
        def _():
            src = seq(i - 1)
            grad_c(src).wait_recv()
            held[src, parts[1]] = jnp.dot(
                grad[src, parts[1]], in_buf[...], preferred_element_type=jnp.float32
            )

            @pl.when(head(src))
            def _():
                relay(src, 1)

        @pl.when(i < n)
        def _():
            src = seq(i)

            @pl.when(jnp.logical_not(head(src)))
            def _():
                relay(src, 0)

        @pl.when(i >= LAG)
        def _():
            src = seq(i - LAG)

            @pl.when(jnp.logical_not(head(src)))
            def _():
                relay(src, 1)

        return carry

    lax.fori_loop(0, n + LAG - 1, step, 0)

    for k in range(deep):
        up_y(2 * k + 1 - y).wait_recv()
    gi = jnp.zeros(gi_ref.shape, jnp.float32)
    for block in range(n):
        gi = gi + lax.dot_general(
            grad[block], up_buf[block], (((0,), (0,)), ((), ())),
            preferred_element_type=jnp.float32,
        )
    gi_ref[...] = gi.astype(gi_ref.dtype)
    relay(f, 1)

    root = jnp.sqrt(jnp.float32(token_total))
    y_copy(0).wait_recv()
    gu_ref[lower] = (held[f, first] + y_in[first].astype(jnp.float32)) / root
    y_copy(1).wait_recv()
    gu_ref[other] = (held[f, second] + y_in[second].astype(jnp.float32)) / root
    gu_ref[middle] = (held[f, last] + y_in[last].astype(jnp.float32)) / root

    swap_copy().wait_send()
    for slot, (src_t, tp) in enumerate(((t, t_core), (t, t_x), (t_x, t_core))):
        cot_copy(src_t, slot, tp).wait_send()
    for k in range(2):
        forward_down(f, k, (-1, 1), finish)
        down_c(f_y, k).wait_send()
    for step_ in (-1, 1):
        @pl.when(inside(z + step_))
        def _():
            up_z(f, step_).wait_send()
    up_y(f).wait_send()
    for d in range(1, deep):
        for sign in (-1, 1):
            @pl.when(inside(z + sign * d))
            def _():
                src = f + 2 * sign * d
                for k in range(2):
                    forward_down(src, k, (-sign,), finish)
                    down_c(f_y + 2 * sign * d, k).wait_send()
                up_y(src).wait_send()

                @pl.when(inside(z - sign))
                def _():
                    up_z(src, -sign).wait_send()

    def drain(src, carry):
        grad_x(src).wait_send()
        grad_c(src).wait_send()
        for part in range(2):
            @pl.when(src // 2 > z)
            def _():
                sum_copy(src, part, 1).wait_send()

            @pl.when(src // 2 < z)
            def _():
                sum_copy(src, part, -1).wait_send()

        return carry

    lax.fori_loop(0, n, drain, 0)
    for part in range(2):
        y_copy(part).wait_send()


def settle(gi_ref, gu_ref, gi_out, gu_out):
    gi_out[...] = gi_ref[...]
    gu_out[...] = gu_ref[...]


def fused(n, tp, cotangent, inputs, pre_act, w_up, w_down):
    tokens, width = cotangent.shape
    rows = w_down.shape[0]
    own_rows = (rows - MIDDLE) // 2 + MIDDLE
    deep = n // 2
    dma = pltpu.SemaphoreType.DMA
    vmem = pl.BlockSpec(memory_space=pltpu.VMEM)
    anywhere = pl.BlockSpec(memory_space=pl.ANY)
    shapes = (
        jax.ShapeDtypeStruct((tokens, width), jnp.bfloat16),
        jax.ShapeDtypeStruct((rows, width), jnp.float32),
    )
    results = pl.pallas_call(
        functools.partial(kernel, n, tokens * n),
        out_shape=shapes,
        in_specs=[anywhere] * 5,
        out_specs=(vmem, vmem),
        scratch_shapes=[
            pltpu.VMEM((tokens, tp * width), jnp.bfloat16),
            pltpu.VMEM((tp * width, tokens), jnp.bfloat16),
            pltpu.VMEM((tokens, width), jnp.bfloat16),
            pltpu.VMEM((n, own_rows, tp * width), jnp.bfloat16),
            pltpu.VMEM((own_rows, width), jnp.bfloat16),
            pltpu.VMEM((n, rows, width), jnp.bfloat16),
            pltpu.VMEM((n, own_rows, tokens), jnp.bfloat16),
            pltpu.VMEM((n, rows, tokens), jnp.bfloat16),
            pltpu.VMEM((n, rows, width), jnp.float32),
            pltpu.VMEM((n, rows, width), jnp.bfloat16),
            pltpu.VMEM((2, n, rows, width), jnp.bfloat16),
            pltpu.VMEM((rows, width), jnp.bfloat16),
            dma((11,)),
            dma((3,)), dma((tp,)), dma((1,)),
            dma((2, deep, 2)), dma((deep, 2)), dma((n, 2)), dma((n, tp)),
            dma((2, deep)), dma((deep,)), dma((n,)),
            dma((n,)), dma((n,)), dma((n,)), dma((n,)),
            dma((n, 2)), dma((2, n, 2)), dma((2,)),
        ],
        compiler_params=pltpu.CompilerParams(
            collective_id=0, has_side_effects=True, vmem_limit_bytes=60 * 2**20
        ),
    )(cotangent, inputs, pre_act.T.reshape(n, rows, tokens), w_up, w_down)
    return pl.pallas_call(
        settle, out_shape=shapes, in_specs=[vmem, vmem], out_specs=(vmem, vmem)
    )(*results)


def gathered(cotangent, inputs, pre_act, w_up, w_down):
    token_total = cotangent.shape[0] * lax.axis_size("fs")
    full_cotangent = lax.all_gather(cotangent, "tp", axis=1, tiled=True)
    down_whole = lax.all_gather(w_down, "tp", axis=1, tiled=True)
    grad_hidden = times_rows(full_cotangent, lax.all_gather(down_whole, "fs", axis=0, tiled=True))
    grad_pre = (2.0 * grad_hidden * jnp.maximum(pre_act.astype(jnp.float32), 0.0)).astype(
        jnp.bfloat16
    )
    grad_input = jnp.dot(
        grad_pre, lax.all_gather(w_up, "fs", axis=0, tiled=True), preferred_element_type=jnp.float32
    )
    grad_share = lax.psum_scatter(
        lax.dot_general(
            grad_pre, inputs, (((0,), (0,)), ((), ())), preferred_element_type=jnp.float32
        ),
        "fs",
        scatter_dimension=0,
        tiled=True,
    )
    grad_up = grad_share / jnp.sqrt(jnp.float32(token_total))
    return (grad_input.astype(jnp.bfloat16), grad_up)


def solution(mesh):
    n, tp = mesh.shape["fs"], mesh.shape["tp"]

    def local(cotangent, inputs, pre_act, w_up, w_down):
        rows, width = w_down.shape
        fits = tp == 4 and n == 8 and rows % 128 == MIDDLE and width % 128 == 0
        if fits:
            return fused(n, tp, cotangent, inputs, pre_act, w_up, w_down)
        return gathered(cotangent, inputs, pre_act, w_up, w_down)

    return jax.shard_map(
        local,
        mesh=mesh,
        in_specs=(P("fs", "tp"), P("fs", "tp"), P("fs", None), P("fs", "tp"), P("fs", "tp")),
        out_specs=(P("fs", "tp"), P("fs", "tp")),
        check_vma=False,
    )
```

time: 56.9 us -> 54.3 us (0.954)
  Pallas kernels: 56.1 us -> 53.5 us
    pallas_call x1, Pallas kernels: 54.2 us -> 51.6 us  [fused(): pl.pallas_call(functools.partial(kernel, n, tokens * n), out_shape=shapes...]
where the time goes in v1:
time: 54.3 us; the launch traced here: 54.1 us
  Pallas kernels  53.5 us (99%)
  between operations  0.64 us (1%)
    pallas_call x1, Pallas kernels, fused(): pl.pallas_call(functools.partial(kernel, n, tokens * n), out_shape=shapes...  51.6 us
    pallas_call x1, Pallas kernels, fused(): pl.pallas_call(settle, out_shape=shapes, in_specs=[vmem, vmem], out_specs...  1.89 us

profile of v1, /device:TPU:0, one launch (start us, length us, event | category | flops | bytes accessed | tf_op | source)
XLA Modules:
  0.0 54.1 jit_solution(9768310881819803695)
XLA Ops:
  0.6 51.6 %shard_map.68 = (bf16[640,256]{1,0:T(8,128)(2,1)}, f32[264,256]{1,0:T(8,128)}) custom-call(bf16[640,256]{1,0:T(8,128)(2,1)} %cot_hbm.1, bf16[640,256]{1,0:T(8,128)(2,1)} %in_hbm.1, bf16[8,264,640]{2,1,0:T(8,128)(2,1)} %bitcast.3, bf16[264,256]{1,0:T(8,128)(2,1)} %up_hbm.1, bf16[264,256]{1,0:T(8,128)(2,1)} %down_hbm.1), custom_call_target="tpu_custom_call" | custom-call | tf_op jit(solution)/shard_map/pallas_call | solution.py:424
  52.2 1.9 %shard_map.69 = (bf16[640,256]{1,0:T(8,128)(2,1)}, f32[264,256]{1,0:T(8,128)}) custom-call(bf16[640,256]{1,0:T(8,128)(2,1)} %get-tuple-element.4.gi_ref, f32[264,256]{1,0:T(8,128)} %get-tuple-element.5.gu_ref), custom_call_target="tpu_custom_call" | custom-call | tf_op jit(solution)/shard_map/pallas_call | solution.py:453

commit v2 on v1

v2 whole, which is shorter than its diff:
```python
import functools

import jax
import jax.numpy as jnp
from jax import lax
from jax.experimental import pallas as pl
from jax.experimental.pallas import tpu as pltpu
from jax.sharding import PartitionSpec as P

MESH = pl.DeviceIdType.MESH
MIDDLE = 8
PU = (0, 1, 4)


def times_rows(left, piece):
    return lax.dot_general(
        left, piece, (((1,), (1,)), ((), ())), preferred_element_type=jnp.float32
    )


def toggled(index, mask, bits):
    for bit in range(bits):
        unit = 2**bit
        index = index + unit * ((mask // unit) % 2) * (1 - 2 * ((index // unit) % 2))
    return index


def kernel(
    n, token_total,
    cot_hbm, in_hbm, pre_hbm, up_hbm, down_hbm,
    gi_ref, gu_ref,
    cot_buf, cot_turned, in_buf, down_buf, swap_buf, up_buf, pre_buf, grad, held,
    y_out, y_in, z_out, z_in,
    local_sem, cot_send, cot_recv, swap_send, dz_send, dy_send, dc_send, down_recv,
    uz_send, uy_send, up_recv, rest_send, rest_recv, gx_send, gx_recv, gc_send, gc_recv,
    ys_send, ys_recv, zs_send, zs_recv,
):
    deep = n // 2
    bits = n.bit_length() - 1
    f = lax.axis_index("fs")
    t = lax.axis_index("tp")
    z, y = f // 2, f % 2
    x, c = t // 2, t % 2
    width = in_buf.shape[1]
    rows = up_buf.shape[1]
    main = (rows - MIDDLE) // 2
    half = main // 2
    own_rows = main + MIDDLE
    t_core = t + 1 - 2 * c
    t_x = t + 2 - 4 * x
    t_xcore = t_core + 2 - 4 * x
    f_y = f + 1 - 2 * y
    is_mid = (z > 0) & (z < deep - 1)

    def cols(tp):
        return pl.ds(pl.multiple_of(tp * width, width), width)

    def far(m):
        return toggled(f, 2 * m, bits)

    def seq(i):
        pair = i // 2
        return toggled(f, 2 * ((pair + 1) % deep) + (i + 1) % 2, bits)

    def remote(src, dst, send, recv, fs, tp):
        return pltpu.make_async_remote_copy(
            src_ref=src, dst_ref=dst, send_sem=send, recv_sem=recv,
            device_id=(fs, tp), device_id_type=MESH,
        )

    lower = pl.ds(pl.multiple_of((main + MIDDLE) * x, 8), main)
    other = pl.ds(pl.multiple_of((main + MIDDLE) * (1 - x), 8), main)
    middle = pl.ds(main, MIDDLE)
    first, second, last = pl.ds(0, main), pl.ds(main, main), pl.ds(2 * main, MIDDLE)
    parts = (first, pl.ds(main, own_rows))

    plan = [
        (down_hbm.at[other], swap_buf.at[first]),
        (down_hbm.at[middle], swap_buf.at[middle]),
        (down_hbm.at[lower], down_buf.at[f, first, cols(t)]),
        (down_hbm.at[middle], down_buf.at[f, middle, cols(t)]),
        (cot_hbm, cot_buf.at[:, cols(t)]),
        (up_hbm.at[lower], up_buf.at[f, first]),
        (up_hbm.at[other], up_buf.at[f, second]),
        (up_hbm.at[middle], up_buf.at[f, last]),
        (in_hbm, in_buf),
        (pre_hbm.at[:, lower], pre_buf.at[:, first]),
        (pre_hbm.at[:, middle], pre_buf.at[:, middle]),
    ]
    local = [
        pltpu.make_async_copy(src, dst, local_sem.at[k]) for k, (src, dst) in enumerate(plan)
    ]
    for copy in local:
        copy.start()

    def swap_copy():
        return remote(
            swap_buf, down_buf.at[f, :, cols(t)], swap_send.at[0], down_recv.at[f, t], f, t_x
        )

    def cot_copy(src_t, slot, tp):
        block = cot_buf.at[:, cols(src_t)]
        return remote(block, block, cot_send.at[slot], cot_recv.at[src_t], f, tp)

    def piece(k):
        return t if k == 0 else t_x

    def down_copy(src_f, k, send, fs, tp):
        block = down_buf.at[src_f, :, cols(piece(k))]
        return remote(block, block, send, down_recv.at[src_f, piece(k)], fs, tp)

    def down_z(src_f, k, step):
        return down_copy(src_f, k, dz_send.at[(1 + step) // 2, src_f // 2, k], f + 2 * step, t)

    def down_y(src_f, k):
        return down_copy(src_f, k, dy_send.at[src_f // 2, k], f_y, t)

    def down_c(src_f, k):
        return down_copy(src_f, k, dc_send.at[src_f, k], f, t_core)

    def up_copy(src_f, area, send, recv, fs):
        block = up_buf.at[src_f, area]
        return remote(block, block, send, recv.at[src_f], fs, t)

    def up_z(m):
        return up_copy(f, pl.ds(0, rows), uz_send.at[m], up_recv, far(m))

    def rest_z(m):
        return up_copy(f_y, parts[1], rest_send.at[m], rest_recv, far(m))

    def up_y(src_f):
        return up_copy(src_f, parts[0], uy_send.at[src_f // 2], up_recv, f_y)

    def rest_y():
        return up_copy(f, parts[1], uy_send.at[deep], rest_recv, f_y)

    def grad_x(src_f):
        src = grad.at[src_f, pl.ds(pl.multiple_of(half * c, half), half)]
        dst = grad.at[src_f, pl.ds(pl.multiple_of(main + half * c, half), half)]
        return remote(src, dst, gx_send.at[src_f], gx_recv.at[src_f], f, t_x)

    def grad_c(src_f):
        block = grad.at[src_f, pl.ds(pl.multiple_of(main + half * c, half), half)]
        return remote(block, block, gc_send.at[src_f], gc_recv.at[src_f], f, t_core)

    def y_copy(pair, part):
        return remote(
            y_out.at[pair, parts[part]], y_in.at[pair, parts[part]],
            ys_send.at[pair, part], ys_recv.at[pair, part], f_y, t,
        )

    def z_copy(pair, part):
        return remote(
            z_out.at[pair, parts[part]], z_in.at[pair, parts[part]],
            zs_send.at[pair, part], zs_recv.at[pair, part], far(pair + 1), t,
        )

    def inside(zz):
        return (zz >= 0) & (zz < deep)

    barrier = pltpu.get_barrier_semaphore()
    peers = [(far(m), t) for m in range(1, deep)] + [(f_y, t), (f, t_core), (f, t_x)]
    for peer in peers:
        pl.semaphore_signal(barrier, inc=1, device_id=peer, device_id_type=MESH)
    for k in range(8):
        local[k].wait()
    pl.semaphore_wait(barrier, len(peers))

    def arrived_down(src_f, tp):
        block = down_buf.at[src_f, :, cols(tp)]
        remote(block, block, swap_send.at[0], down_recv.at[src_f, tp], f, t_core).wait_recv()

    def arrived_cot(src_t):
        cot_copy(src_t, 0, t_core).wait_recv()

    def forward_down(src_f, k, steps, act):
        for step in steps:
            @pl.when(inside(z + step))
            def _():
                act(down_z(src_f, k, step))
        act(down_y(src_f, k))
        act(down_c(src_f, k))

    def start(copy):
        copy.start()

    def finish(copy):
        copy.wait_send()

    def line(d, k):
        for sign in (-1, 1):
            @pl.when(inside(z + sign * d))
            def _():
                src = f + 2 * sign * d
                arrived_down(src, piece(k))
                forward_down(src, k, (-sign,), start)

    def beside(d, k):
        for sign in (-1, 1) if d else (1,):
            @pl.when(inside(z + sign * d))
            def _():
                src = f_y + 2 * sign * d
                arrived_down(src, piece(k))
                down_c(src, k).start()

    def offer_up():
        up_z(2).start()
        up_z(1).start()

        @pl.when(is_mid)
        def _():
            up_z(3).start()

        up_copy(f_y, parts[1], uy_send.at[deep], rest_recv, f_y).wait_recv()
        rest_z(2).start()
        rest_z(1).start()

        @pl.when(is_mid)
        def _():
            rest_z(3).start()

    def turn(tp):
        cot_turned[cols(tp)] = cot_buf[:, cols(tp)].T

    swap_copy().start()
    forward_down(f, 0, (-1, 1), start)
    rest_y().start()
    cot_copy(t, 1, t_x).start()
    cot_copy(t, 0, t_core).start()
    turn(t)
    arrived_down(f, t_x)
    forward_down(f, 1, (-1, 1), start)
    line(1, 0)
    beside(0, 0)
    for k in range(8, len(local)):
        local[k].wait()
    arrived_cot(t_core)
    turn(t_core)
    line(1, 1)
    beside(0, 1)
    line(2, 0)
    beside(1, 0)
    line(2, 1)
    offer_up()
    line(3, 0)
    beside(1, 1)
    beside(2, 0)
    arrived_cot(t_x)
    cot_copy(t_x, 2, t_core).start()
    turn(t_x)
    arrived_cot(t_xcore)
    turn(t_xcore)

    def share(pair, part, across, value):
        if across:
            y_out[pair, parts[part]] = value.astype(jnp.bfloat16)
            y_copy(pair, part).start()
        else:
            held[pair, parts[part]] = value

    def combine(pair, part):
        y_copy(pair, part).wait_recv()
        area = parts[part]
        z_out[pair, area] = (
            held[pair, area] + y_in[pair, area].astype(jnp.float32)
        ).astype(jnp.bfloat16)
        z_copy(pair, part).start()

    def produce(pair):
        for across in (1, 0):
            src = seq(2 * pair + 1 - across)
            arrived_down(src, t_core)
            arrived_down(src, t_xcore)
            hidden = jnp.dot(down_buf[src], cot_turned[...], preferred_element_type=jnp.float32)
            grad_pre = (
                2.0 * hidden * jnp.maximum(pre_buf[src].astype(jnp.float32), 0.0)
            ).astype(jnp.bfloat16)
            grad[src, first] = grad_pre[:main]
            grad[src, last] = grad_pre[main:]
            grad_x(src).start()
            share(pair, 0, across, jnp.dot(
                grad_pre[:main], in_buf[...], preferred_element_type=jnp.float32
            ))

    def produce_step(pair, carry):
        @pl.when(pair == 1)
        def _():
            line(3, 1)
            beside(2, 1)
            beside(3, 0)
            up_y(f).start()

        @pl.when(pair == 2)
        def _():
            beside(3, 1)

        produce(pair)
        return carry

    lax.fori_loop(0, deep, produce_step, 0)

    def relays():
        return (
            up_copy(far(2), pl.ds(0, rows), uz_send.at[0], up_recv, far(1)),
            up_copy(toggled(f, 5, bits), parts[1], rest_send.at[0], rest_recv, far(1)),
        )

    def pass_up(m):
        up_copy(far(m), pl.ds(0, rows), uz_send.at[m], up_recv, f_y).wait_recv()
        if m == 2:
            @pl.when(is_mid)
            def _():
                whole, rest = relays()
                whole.start()
                rest.wait_recv()
                rest.start()

        up_y(far(m)).start()

    def step(i, carry):
        @pl.when(i < n)
        def _():
            src = seq(i)
            grad_x(src).wait_recv()
            grad_c(src).start()

        @pl.when((i > 0) & (i <= n))
        def _():
            j = i - 1
            src = seq(j)
            pair = j // 2
            grad_c(src).wait_recv()
            part = jnp.dot(
                grad[src, parts[1]], in_buf[...], preferred_element_type=jnp.float32
            )

            @pl.when(j % 2 == 0)
            def _():
                share(pair, 1, 1, part)

            @pl.when(j % 2 == 1)
            def _():
                share(pair, 1, 0, part)

        @pl.when(i < deep - 1)
        def _():
            combine(i, 0)

        @pl.when((i % 2 == 1) & (i >= 3) & (i < 2 * deep))
        def _():
            combine((i - 3) // 2, 1)

        for k, m in ((PU[0], 2), (PU[1], 1), (PU[2], 3)):
            @pl.when(i == k)
            def _():
                pass_up(m)

        return carry

    lax.fori_loop(0, n + 1, step, 0)

    for m in range(deep):
        src = toggled(f, 2 * m + 1, bits)
        up_y(src).wait_recv()
        rest = up_copy(src, parts[1], uy_send.at[deep], rest_recv, f_y)
        if m == 2:
            @pl.when(jnp.logical_not(is_mid))
            def _():
                rest.wait_recv()
        elif m:
            rest.wait_recv()
    gi = jnp.zeros(gi_ref.shape, jnp.float32)
    for block in range(n):
        gi = gi + lax.dot_general(
            grad[block], up_buf[block], (((0,), (0,)), ((), ())),
            preferred_element_type=jnp.float32,
        )
    gi_ref[...] = gi.astype(gi_ref.dtype)

    root = jnp.sqrt(jnp.float32(token_total))
    for part, area in enumerate(parts):
        total = held[deep - 1, area]
        for pair in range(deep - 1):
            z_copy(pair, part).wait_recv()
            total = total + z_in[pair, area].astype(jnp.float32)
        y_copy(deep - 1, part).wait_recv()
        total = (total + y_in[deep - 1, area].astype(jnp.float32)) / root
        if part == 0:
            gu_ref[lower] = total
        else:
            gu_ref[other] = total[:main]
            gu_ref[middle] = total[main:]

    swap_copy().wait_send()
    rest_y().wait_send()
    for slot, (src_t, tp) in enumerate(((t, t_core), (t, t_x), (t_x, t_core))):
        cot_copy(src_t, slot, tp).wait_send()
    for k in range(2):
        forward_down(f, k, (-1, 1), finish)
        down_c(f_y, k).wait_send()
    for m in range(1, deep):
        if m < 3:
            up_z(m).wait_send()
            rest_z(m).wait_send()
        up_y(far(m)).wait_send()

    @pl.when(is_mid)
    def _():
        up_z(3).wait_send()
        rest_z(3).wait_send()
        for copy in relays():
            copy.wait_send()

    up_y(f).wait_send()
    for d in range(1, deep):
        for sign in (-1, 1):
            @pl.when(inside(z + sign * d))
            def _():
                src = f + 2 * sign * d
                for k in range(2):
                    forward_down(src, k, (-sign,), finish)
                    down_c(f_y + 2 * sign * d, k).wait_send()

    def drain(src, carry):
        grad_x(src).wait_send()
        grad_c(src).wait_send()
        return carry

    lax.fori_loop(0, n, drain, 0)
    for part in range(2):
        for pair in range(deep):
            y_copy(pair, part).wait_send()
            if pair < deep - 1:
                z_copy(pair, part).wait_send()


def settle(gi_ref, gu_ref, gi_out, gu_out):
    gi_out[...] = gi_ref[...]
    gu_out[...] = gu_ref[...]


def fused(n, tp, cotangent, inputs, pre_act, w_up, w_down):
    tokens, width = cotangent.shape
    rows = w_down.shape[0]
    own_rows = (rows - MIDDLE) // 2 + MIDDLE
    deep = n // 2
    dma = pltpu.SemaphoreType.DMA
    vmem = pl.BlockSpec(memory_space=pltpu.VMEM)
    anywhere = pl.BlockSpec(memory_space=pl.ANY)
    shapes = (
        jax.ShapeDtypeStruct((tokens, width), jnp.bfloat16),
        jax.ShapeDtypeStruct((rows, width), jnp.float32),
    )
    results = pl.pallas_call(
        functools.partial(kernel, n, tokens * n),
        out_shape=shapes,
        in_specs=[anywhere] * 5,
        out_specs=(vmem, vmem),
        scratch_shapes=[
            pltpu.VMEM((tokens, tp * width), jnp.bfloat16),
            pltpu.VMEM((tp * width, tokens), jnp.bfloat16),
            pltpu.VMEM((tokens, width), jnp.bfloat16),
            pltpu.VMEM((n, own_rows, tp * width), jnp.bfloat16),
            pltpu.VMEM((own_rows, width), jnp.bfloat16),
            pltpu.VMEM((n, rows, width), jnp.bfloat16),
            pltpu.VMEM((n, own_rows, tokens), jnp.bfloat16),
            pltpu.VMEM((n, rows, tokens), jnp.bfloat16),
            pltpu.VMEM((deep, rows, width), jnp.float32),
            pltpu.VMEM((deep, rows, width), jnp.bfloat16),
            pltpu.VMEM((deep, rows, width), jnp.bfloat16),
            pltpu.VMEM((deep - 1, rows, width), jnp.bfloat16),
            pltpu.VMEM((deep - 1, rows, width), jnp.bfloat16),
            dma((11,)),
            dma((3,)), dma((tp,)), dma((1,)),
            dma((2, deep, 2)), dma((deep, 2)), dma((n, 2)), dma((n, tp)),
            dma((deep,)), dma((deep + 1,)), dma((n,)), dma((deep,)), dma((n,)),
            dma((n,)), dma((n,)), dma((n,)), dma((n,)),
            dma((deep, 2)), dma((deep, 2)), dma((deep - 1, 2)), dma((deep - 1, 2)),
        ],
        compiler_params=pltpu.CompilerParams(
            collective_id=0, has_side_effects=True, vmem_limit_bytes=60 * 2**20
        ),
    )(cotangent, inputs, pre_act.T.reshape(n, rows, tokens), w_up, w_down)
    return pl.pallas_call(
        settle, out_shape=shapes, in_specs=[vmem, vmem], out_specs=(vmem, vmem)
    )(*results)


def gathered(cotangent, inputs, pre_act, w_up, w_down):
    token_total = cotangent.shape[0] * lax.axis_size("fs")
    full_cotangent = lax.all_gather(cotangent, "tp", axis=1, tiled=True)
    down_whole = lax.all_gather(w_down, "tp", axis=1, tiled=True)
    grad_hidden = times_rows(full_cotangent, lax.all_gather(down_whole, "fs", axis=0, tiled=True))
    grad_pre = (2.0 * grad_hidden * jnp.maximum(pre_act.astype(jnp.float32), 0.0)).astype(
        jnp.bfloat16
    )
    grad_input = jnp.dot(
        grad_pre, lax.all_gather(w_up, "fs", axis=0, tiled=True), preferred_element_type=jnp.float32
    )
    grad_share = lax.psum_scatter(
        lax.dot_general(
            grad_pre, inputs, (((0,), (0,)), ((), ())), preferred_element_type=jnp.float32
        ),
        "fs",
        scatter_dimension=0,
        tiled=True,
    )
    grad_up = grad_share / jnp.sqrt(jnp.float32(token_total))
    return (grad_input.astype(jnp.bfloat16), grad_up)


def solution(mesh):
    n, tp = mesh.shape["fs"], mesh.shape["tp"]

    def local(cotangent, inputs, pre_act, w_up, w_down):
        rows, width = w_down.shape
        fits = tp == 4 and n == 8 and rows % 128 == MIDDLE and width % 128 == 0
        if fits:
            return fused(n, tp, cotangent, inputs, pre_act, w_up, w_down)
        return gathered(cotangent, inputs, pre_act, w_up, w_down)

    return jax.shard_map(
        local,
        mesh=mesh,
        in_specs=(P("fs", "tp"), P("fs", "tp"), P("fs", None), P("fs", "tp"), P("fs", "tp")),
        out_specs=(P("fs", "tp"), P("fs", "tp")),
        check_vma=False,
    )
```

time: 54.3 us -> 50.9 us (0.937)
  Pallas kernels: 53.5 us -> 50.1 us
    pallas_call x1, Pallas kernels: 51.6 us -> 48.2 us  [fused(): pl.pallas_call(functools.partial(kernel, n, tokens * n), out_shape=shapes...]
where the time goes in v2:
time: 50.9 us; the launch traced here: 50.7 us
  Pallas kernels  50.1 us (98%)
  between operations  0.64 us (1%)
    pallas_call x1, Pallas kernels, fused(): pl.pallas_call(functools.partial(kernel, n, tokens * n), out_shape=shapes...  48.2 us
    pallas_call x1, Pallas kernels, fused(): pl.pallas_call(settle, out_shape=shapes, in_specs=[vmem, vmem], out_specs...  1.89 us

profile of v2, /device:TPU:0, one launch (start us, length us, event | category | flops | bytes accessed | tf_op | source)
XLA Modules:
  0.0 50.7 jit_solution(14363140157182904047)
XLA Ops:
  0.6 48.2 %shard_map.68 = (bf16[640,256]{1,0:T(8,128)(2,1)}, f32[264,256]{1,0:T(8,128)}) custom-call(bf16[640,256]{1,0:T(8,128)(2,1)} %cot_hbm.1, bf16[640,256]{1,0:T(8,128)(2,1)} %in_hbm.1, bf16[8,264,640]{2,1,0:T(8,128)(2,1)} %bitcast.3, bf16[264,256]{1,0:T(8,128)(2,1)} %up_hbm.1, bf16[264,256]{1,0:T(8,128)(2,1)} %down_hbm.1), custom_call_target="tpu_custom_call" | custom-call | tf_op jit(solution)/shard_map/pallas_call | solution.py:454
  48.8 1.9 %shard_map.69 = (bf16[640,256]{1,0:T(8,128)(2,1)}, f32[264,256]{1,0:T(8,128)}) custom-call(bf16[640,256]{1,0:T(8,128)(2,1)} %get-tuple-element.4.gi_ref, f32[264,256]{1,0:T(8,128)} %get-tuple-element.5.gu_ref), custom_call_target="tpu_custom_call" | custom-call | tf_op jit(solution)/shard_map/pallas_call | solution.py:484

commit v3 on v2

--- a/solution.py
+++ b/solution.py
@@ -9,7 +9,18 @@
 
 MESH = pl.DeviceIdType.MESH
 MIDDLE = 8
-PU = (0, 1, 4)
+ORDER = (
+    ("uz", 1), ("rest",), ("cots",), ("line", 1, 0), ("core",), ("own",), ("rz", 3),
+    ("line", 3, 0), ("line", 2, 0), ("line", 1, 1), ("uz", 3), ("rz", 2), ("cot",),
+    ("line", 3, 1), ("uz", 2), ("line", 2, 1), ("beside", 0, 1), ("both",), ("beside", 0, 0),
+    ("beside", 2, 0), ("make", 1), ("make", 6), ("beside", 1, 1), ("beside", 1, 0), ("make", 0),
+    ("beside", 3, 0), ("beside", 3, 1), ("make", 4), ("beside", 2, 1), ("ufy", 1), ("rz", 1),
+    ("make", 2), ("make", 3), ("make", 5), ("comb", 0, 0), ("gx", 1), ("comb", 2, 0), ("gx", 6),
+    ("up",), ("gx", 0), ("make", 7), ("gx", 4), ("rrel",), ("more", 0), ("comb", 1, 0),
+    ("gx", 2), ("more", 4), ("gx", 3), ("more", 1), ("more", 2), ("ufy", 2), ("more", 3),
+    ("urel",), ("comb", 0, 1), ("gx", 5), ("ufy", 3), ("more", 5), ("comb", 2, 1), ("gx", 7),
+    ("comb", 1, 1), ("more", 6), ("more", 7),
+)
 
 
 def times_rows(left, piece):
@@ -159,12 +170,16 @@
         return (zz >= 0) & (zz < deep)
 
     barrier = pltpu.get_barrier_semaphore()
-    peers = [(far(m), t) for m in range(1, deep)] + [(f_y, t), (f, t_core), (f, t_x)]
-    for peer in peers:
+    for peer in ((f_y, t), (f, t_core), (f, t_x)):
         pl.semaphore_signal(barrier, inc=1, device_id=peer, device_id_type=MESH)
+    for step in (-1, 1):
+        @pl.when(inside(z + step))
+        def _():
+            pl.semaphore_signal(barrier, inc=1, device_id=(f + 2 * step, t), device_id_type=MESH)
+
     for k in range(8):
         local[k].wait()
-    pl.semaphore_wait(barrier, len(peers))
+    pl.semaphore_wait(barrier, 4 + is_mid.astype(jnp.int32))
 
     def arrived_down(src_f, tp):
         block = down_buf.at[src_f, :, cols(tp)]
@@ -187,69 +202,14 @@
     def finish(copy):
         copy.wait_send()
 
-    def line(d, k):
-        for sign in (-1, 1):
-            @pl.when(inside(z + sign * d))
-            def _():
-                src = f + 2 * sign * d
-                arrived_down(src, piece(k))
-                forward_down(src, k, (-sign,), start)
-
-    def beside(d, k):
-        for sign in (-1, 1) if d else (1,):
-            @pl.when(inside(z + sign * d))
-            def _():
-                src = f_y + 2 * sign * d
-                arrived_down(src, piece(k))
-                down_c(src, k).start()
-
-    def offer_up():
-        up_z(2).start()
-        up_z(1).start()
-
-        @pl.when(is_mid)
-        def _():
-            up_z(3).start()
-
-        up_copy(f_y, parts[1], uy_send.at[deep], rest_recv, f_y).wait_recv()
-        rest_z(2).start()
-        rest_z(1).start()
-
-        @pl.when(is_mid)
-        def _():
-            rest_z(3).start()
+    def arrived_up(src_f):
+        up_copy(src_f, pl.ds(0, rows), uz_send.at[0], up_recv, f_y).wait_recv()
+
+    def arrived_rest(src_f):
+        up_copy(src_f, parts[1], uy_send.at[deep], rest_recv, f_y).wait_recv()
 
     def turn(tp):
         cot_turned[cols(tp)] = cot_buf[:, cols(tp)].T
-
-    swap_copy().start()
-    forward_down(f, 0, (-1, 1), start)
-    rest_y().start()
-    cot_copy(t, 1, t_x).start()
-    cot_copy(t, 0, t_core).start()
-    turn(t)
-    arrived_down(f, t_x)
-    forward_down(f, 1, (-1, 1), start)
-    line(1, 0)
-    beside(0, 0)
-    for k in range(8, len(local)):
-        local[k].wait()
-    arrived_cot(t_core)
-    turn(t_core)
-    line(1, 1)
-    beside(0, 1)
-    line(2, 0)
-    beside(1, 0)
-    line(2, 1)
-    offer_up()
-    line(3, 0)
-    beside(1, 1)
-    beside(2, 0)
-    arrived_cot(t_x)
-    cot_copy(t_x, 2, t_core).start()
-    turn(t_x)
-    arrived_cot(t_xcore)
-    turn(t_xcore)
 
     def share(pair, part, across, value):
         if across:
@@ -258,7 +218,124 @@
         else:
             held[pair, parts[part]] = value
 
-    def combine(pair, part):
+    def relay_up():
+        return up_copy(far(2), pl.ds(0, rows), uz_send.at[0], up_recv, far(1))
+
+    def relay_rest():
+        return up_copy(toggled(f, 5, bits), parts[1], rest_send.at[0], rest_recv, far(1))
+
+    seen = set()
+
+    def once(name, act):
+        if name not in seen:
+            seen.add(name)
+            act()
+
+    def do_own():
+        arrived_down(f, t_x)
+        forward_down(f, 1, (-1, 1), start)
+
+    def do_line(m, k):
+        src = far(m)
+        arrived_down(src, piece(k))
+        for step in (-1, 1):
+            @pl.when(inside(z + step) & ((src < f) == (step > 0)))
+            def _():
+                down_z(src, k, step).start()
+
+        down_y(src, k).start()
+        down_c(src, k).start()
+
+    def do_beside(m, k):
+        src = toggled(f, 2 * m + 1, bits)
+        arrived_down(src, piece(k))
+        down_c(src, k).start()
+
+    def do_cots():
+        cot_copy(t, 1, t_x).start()
+        cot_copy(t, 0, t_core).start()
+        turn(t)
+
+    def do_cot_core():
+        arrived_cot(t_core)
+        turn(t_core)
+
+    def do_cot_x():
+        arrived_cot(t_x)
+        cot_copy(t_x, 2, t_core).start()
+        turn(t_x)
+
+    def do_cot_xc():
+        arrived_cot(t_xcore)
+        turn(t_xcore)
+
+    def do_uz(m):
+        if m < 3:
+            up_z(m).start()
+        else:
+            @pl.when(is_mid)
+            def _():
+                up_z(3).start()
+
+    def do_rz(m):
+        once("rest", lambda: arrived_rest(f_y))
+        if m < 3:
+            rest_z(m).start()
+        else:
+            @pl.when(is_mid)
+            def _():
+                rest_z(3).start()
+
+    def do_ufy(m):
+        once(("up", m), lambda: arrived_up(far(m)))
+        up_y(far(m)).start()
+
+    def do_urel():
+        once(("up", 2), lambda: arrived_up(far(2)))
+
+        @pl.when(is_mid)
+        def _():
+            relay_up().start()
+
+    def do_rrel():
+        @pl.when(is_mid)
+        def _():
+            relay_rest().wait_recv()
+            relay_rest().start()
+
+    def more_local():
+        for k in range(8, len(local)):
+            local[k].wait()
+
+    def do_make(i):
+        once("local", more_local)
+        src = seq(i)
+        arrived_down(src, t_core)
+        arrived_down(src, t_xcore)
+        hidden = jnp.dot(down_buf[src], cot_turned[...], preferred_element_type=jnp.float32)
+        grad_pre = (
+            2.0 * hidden * jnp.maximum(pre_buf[src].astype(jnp.float32), 0.0)
+        ).astype(jnp.bfloat16)
+        grad[src, first] = grad_pre[:main]
+        grad[src, last] = grad_pre[main:]
+        grad_x(src).start()
+        share(i // 2, 0, i % 2 == 0, jnp.dot(
+            grad_pre[:main], in_buf[...], preferred_element_type=jnp.float32
+        ))
+
+    def do_gx(i):
+        src = seq(i)
+        grad_x(src).wait_recv()
+        grad_c(src).start()
+
+    def do_more(i):
+        src = seq(i)
+        grad_c(src).wait_recv()
+        share(i // 2, 1, i % 2 == 0, jnp.dot(
+            grad[src, parts[1]], in_buf[...], preferred_element_type=jnp.float32
+        ))
+
+    def do_comb(pair, part):
         y_copy(pair, part).wait_recv()
         area = parts[part]
         z_out[pair, area] = (
@@ -266,98 +343,17 @@
         ).astype(jnp.bfloat16)
         z_copy(pair, part).start()
 
-    def produce(pair):
-        for across in (1, 0):
-            src = seq(2 * pair + 1 - across)
-            arrived_down(src, t_core)
-            arrived_down(src, t_xcore)
-            hidden = jnp.dot(down_buf[src], cot_turned[...], preferred_element_type=jnp.float32)
-            grad_pre = (
-                2.0 * hidden * jnp.maximum(pre_buf[src].astype(jnp.float32), 0.0)
-            ).astype(jnp.bfloat16)
-            grad[src, first] = grad_pre[:main]
-            grad[src, last] = grad_pre[main:]
-            grad_x(src).start()
-            share(pair, 0, across, jnp.dot(
-                grad_pre[:main], in_buf[...], preferred_element_type=jnp.float32
-            ))
-
-    def produce_step(pair, carry):
-        @pl.when(pair == 1)
-        def _():
-            line(3, 1)
-            beside(2, 1)
-            beside(3, 0)
-            up_y(f).start()
-
-        @pl.when(pair == 2)
-        def _():
-            beside(3, 1)
-
-        produce(pair)
-        return carry
-
-    lax.fori_loop(0, deep, produce_step, 0)
-
-    def relays():
-        return (
-            up_copy(far(2), pl.ds(0, rows), uz_send.at[0], up_recv, far(1)),
-            up_copy(toggled(f, 5, bits), parts[1], rest_send.at[0], rest_recv, far(1)),
-        )
-
-    def pass_up(m):
-        up_copy(far(m), pl.ds(0, rows), uz_send.at[m], up_recv, f_y).wait_recv()
-        if m == 2:
-            @pl.when(is_mid)
-            def _():
-                whole, rest = relays()
-                whole.start()
-                rest.wait_recv()
-                rest.start()
-
-        up_y(far(m)).start()
-
-    def step(i, carry):
-        @pl.when(i < n)
-        def _():
-            src = seq(i)
-            grad_x(src).wait_recv()
-            grad_c(src).start()
-
-        @pl.when((i > 0) & (i <= n))
-        def _():
-            j = i - 1
-            src = seq(j)
-            pair = j // 2
-            grad_c(src).wait_recv()
-            part = jnp.dot(
-                grad[src, parts[1]], in_buf[...], preferred_element_type=jnp.float32
-            )
-
-            @pl.when(j % 2 == 0)
-            def _():
-                share(pair, 1, 1, part)
-
-            @pl.when(j % 2 == 1)
-            def _():
-                share(pair, 1, 0, part)
-
-        @pl.when(i < deep - 1)
-        def _():
-            combine(i, 0)
-
-        @pl.when((i % 2 == 1) & (i >= 3) & (i < 2 * deep))
-        def _():
-            combine((i - 3) // 2, 1)
-
-        for k, m in ((PU[0], 2), (PU[1], 1), (PU[2], 3)):
-            @pl.when(i == k)
-            def _():
-                pass_up(m)
-
-        return carry
-
-    lax.fori_loop(0, n + 1, step, 0)
+    swap_copy().start()
+    forward_down(f, 0, (-1, 1), start)
+    acts = {
+        "own": do_own, "line": do_line, "beside": do_beside, "cots": do_cots,
+        "core": do_cot_core, "cot": do_cot_x, "both": do_cot_xc,
+        "rest": lambda: rest_y().start(), "up": lambda: up_y(f).start(),
+        "uz": do_uz, "rz": do_rz, "ufy": do_ufy, "urel": do_urel, "rrel": do_rrel,
+        "make": do_make, "gx": do_gx, "more": do_more, "comb": do_comb,
+    }
+    for name, *values in ORDER:
+        acts[name](*values)
 
     for m in range(deep):
         src = toggled(f, 2 * m + 1, bits)
@@ -408,8 +404,8 @@
     def _():
         up_z(3).wait_send()
         rest_z(3).wait_send()
-        for copy in relays():
-            copy.wait_send()
+        relay_up().wait_send()
+        relay_rest().wait_send()
 
     up_y(f).wait_send()
     for d in range(1, deep):

time: 50.9 us -> 49 us (0.963)
  Pallas kernels: 50.1 us -> 48.2 us
    pallas_call x1, Pallas kernels: 48.2 us -> 46.3 us  [fused(): pl.pallas_call(functools.partial(kernel, n, tokens * n), out_shape=shapes...]
where the time goes in v3:
time: 49 us; the launch traced here: 48.9 us
  Pallas kernels  48.2 us (98%)
  between operations  0.64 us (1%)
    pallas_call x1, Pallas kernels, fused(): pl.pallas_call(functools.partial(kernel, n, tokens * n), out_shape=shapes...  46.3 us
    pallas_call x1, Pallas kernels, fused(): pl.pallas_call(settle, out_shape=shapes, in_specs=[vmem, vmem], out_specs...  1.89 us

profile of v3, /device:TPU:0, one launch (start us, length us, event | category | flops | bytes accessed | tf_op | source)
XLA Modules:
  0.0 48.9 jit_solution(17092238595468123254)
XLA Ops:
  0.6 46.3 %shard_map.68 = (bf16[640,256]{1,0:T(8,128)(2,1)}, f32[264,256]{1,0:T(8,128)}) custom-call(bf16[640,256]{1,0:T(8,128)(2,1)} %cot_hbm.1, bf16[640,256]{1,0:T(8,128)(2,1)} %in_hbm.1, bf16[8,264,640]{2,1,0:T(8,128)(2,1)} %bitcast.3, bf16[264,256]{1,0:T(8,128)(2,1)} %up_hbm.1, bf16[264,256]{1,0:T(8,128)(2,1)} %down_hbm.1), custom_call_target="tpu_custom_call" | custom-call | tf_op jit(solution)/shard_map/pallas_call | solution.py:450
  47.0 1.9 %shard_map.69 = (bf16[640,256]{1,0:T(8,128)(2,1)}, f32[264,256]{1,0:T(8,128)}) custom-call(bf16[640,256]{1,0:T(8,128)(2,1)} %get-tuple-element.4.gi_ref, f32[264,256]{1,0:T(8,128)} %get-tuple-element.5.gu_ref), custom_call_target="tpu_custom_call" | custom-call | tf_op jit(solution)/shard_map/pallas_call | solution.py:480

commit v4 on v3

--- a/solution.py
+++ b/solution.py
@@ -442,7 +442,7 @@
     deep = n // 2
     dma = pltpu.SemaphoreType.DMA
     vmem = pl.BlockSpec(memory_space=pltpu.VMEM)
-    anywhere = pl.BlockSpec(memory_space=pl.ANY)
+    anywhere = pl.BlockSpec(memory_space=pltpu.HBM)
     shapes = (
         jax.ShapeDtypeStruct((tokens, width), jnp.bfloat16),
         jax.ShapeDtypeStruct((rows, width), jnp.float32),
@@ -474,11 +474,12 @@
             dma((deep, 2)), dma((deep, 2)), dma((deep - 1, 2)), dma((deep - 1, 2)),
         ],
         compiler_params=pltpu.CompilerParams(
-            collective_id=0, has_side_effects=True, vmem_limit_bytes=60 * 2**20
+            collective_id=0, has_side_effects=True, vmem_limit_bytes=24 * 2**20
         ),
-    )(cotangent, inputs, pre_act.T.reshape(n, rows, tokens), w_up, w_down)
+    )(*(pltpu.with_memory_space_constraint(q, pltpu.HBM) for q in (cotangent, inputs, pre_act.T.reshape(n, rows, tokens), w_up, w_down)))
     return pl.pallas_call(
-        settle, out_shape=shapes, in_specs=[vmem, vmem], out_specs=(vmem, vmem)
+        settle, out_shape=shapes, in_specs=[vmem, vmem], out_specs=(vmem, vmem),
+        compiler_params=pltpu.CompilerParams(vmem_limit_bytes=4 * 2**20),
     )(*results)
 
 

time: 49 us -> 47.2 us (0.963)
  Pallas kernels: 48.2 us -> 46.4 us
    pallas_call x1, Pallas kernels: 1.89 us -> 0.85 us  [fused(): pl.pallas_call(settle, out_shape=shapes, in_specs=[vmem, vmem], out_specs...]
    pallas_call x1, Pallas kernels: 46.3 us -> 45.5 us  [fused(): pl.pallas_call(functools.partial(kernel, n, tokens * n), out_shape=shapes...]
where the time goes in v4:
time: 47.2 us; the launch traced here: 47 us
  Pallas kernels  46.4 us (98%)
  between operations  0.64 us (1%)
    pallas_call x1, Pallas kernels, fused(): pl.pallas_call(functools.partial(kernel, n, tokens * n), out_shape=shapes...  45.5 us

profile of v4, /device:TPU:0, one launch (start us, length us, event | category | flops | bytes accessed | tf_op | source)
XLA Modules:
  0.0 47.0 jit_solution(7928900403971518105)
XLA Ops:
  0.6 45.5 %shard_map.68 = (bf16[640,256]{1,0:T(8,128)(2,1)S(1)}, f32[264,256]{1,0:T(8,128)S(1)}) custom-call(bf16[640,256]{1,0:T(8,128)(2,1)} %cot_hbm.1, bf16[640,256]{1,0:T(8,128)(2,1)} %in_hbm.1, bf16[8,264,640]{2,1,0:T(8,128)(2,1)} %bitcast.3, bf16[264,256]{1,0:T(8,128)(2,1)} %up_hbm.1, bf16[264,256]{1,0:T(8,128)(2,1)} %down_hbm.1), custom_call_target="tpu_custom_call" | custom-call | tf_op jit(solution)/shard_map/pallas_call | solution.py:450
  46.2 0.9 %shard_map.69 = (bf16[640,256]{1,0:T(8,128)(2,1)}, f32[264,256]{1,0:T(8,128)}) custom-call(bf16[640,256]{1,0:T(8,128)(2,1)S(1)} %get-tuple-element.4.gi_ref, f32[264,256]{1,0:T(8,128)S(1)} %get-tuple-element.5.gu_ref), custom_call_target="tpu_custom_call" | custom-call | tf_op jit(solution)/shard_map/pallas_call | solution.py:480
